TPU v7x, 32 devices: a whole 2x2x4 slice. The times are simulated.
32 devices in a mesh: rep: 2 (over core), fs: 8 (over z, y), tp: 2 (over x).
Axes of the slice: x: 2, y: 2, z: 4, core: 2. Of those that a mesh axis runs over, the one named last changes fastest.
Arguments:
- residual: bfloat16 [2048, 4096], P('tp', ('rep', 'fs')), may hold values from -6 to 6
- mixer_gain: float32 [2048], replicated, may hold values from 0.1 to 1.9
- value_weight: float32 [2048, 512], P('fs', 'tp'), may hold values from -0.125 to 0.125
- value_scale: float32 [512], P('tp'), may hold values from 0.2 to 8, as said below
- input_gate_weight: float32 [2048, 512], P('fs', 'tp'), may hold values from -0.125 to 0.125
- input_gate_scale: float32 [512], P('tp'), may hold values from 0.5 to 2
- output_gate_weight: float32 [2048, 512], P('fs', 'tp'), may hold values from -0.125 to 0.125
- output_gate_scale: float32 [512], P('tp'), may hold values from 0.5 to 2
- conv_taps: float32 [3, 512], P(None, 'tp'), may hold values from -3 to 3
- conv_gain: float32 [512], P('tp'), may hold values from 0.1 to 1.9
- mixer_out_weight: float32 [512, 2048], P('tp', 'fs'), may hold values from -0.25 to 0.25
- mixer_out_scale: float32 [2048], P('fs'), may hold values from 0.5 to 2
- channel_gain: float32 [2048], replicated, may hold values from 0.1 to 1.9
- gate_weight: float32 [2048, 5632], P('fs', 'tp'), may hold values from -0.125 to 0.125
- gate_scale: float32 [5632], P('tp'), may hold values from 0.5 to 2
- up_weight: float32 [2048, 5632], P('fs', 'tp'), may hold values from -0.125 to 0.125
- up_scale: float32 [5632], P('tp'), may hold values from 0.5 to 2
- down_weight: float32 [5632, 2048], P('tp', 'fs'), may hold values from -0.078125 to 0.078125
- down_scale: float32 [2048], P('fs'), may hold values from 0.5 to 2
Outputs:
- layer_out: bfloat16 [2048, 4096], P('tp', ('rep', 'fs'))
Inputs may be any that keep to these rules, and one draw needn't show every extreme that they name: `value_scale`: positive column scales.
All inputs are finite; a program needn't handle non-finite values.
Results may differ from a plain program's by a relative error of at most 0.018.
Values may be sent and summed in bfloat16 or wider, within the bound.
A program may use at most 128 MiB of HBM per device.

v0:
```python
import functools

import jax
import jax.numpy as jnp
from jax import lax
from jax.experimental import pallas as pl
from jax.experimental.pallas import tpu as pltpu
from jax.sharding import PartitionSpec as P

LEN = 128
MESH = pl.DeviceIdType.MESH

epsilon = 1e-06


def contract(weight, rows):
    return lax.dot_general(
        weight, rows, (((0,), (0,)), ((), ())), preferred_element_type=jnp.float32
    )


def normalize(values, gain):
    floats = values.astype(jnp.float32)
    mean = jnp.mean(floats * floats, axis=0, keepdims=True)
    return (floats * lax.rsqrt(mean + epsilon) * gain[:, None]).astype(jnp.bfloat16)


def causal_conv(values, taps, length):
    total = values.shape[1]
    position = jnp.arange(total, dtype=jnp.int32) % length
    shifted_one = jnp.pad(values, ((0, 0), (1, 0)))[:, :total]
    shifted_two = jnp.pad(values, ((0, 0), (2, 0)))[:, :total]
    shifted_one = jnp.where(position[None, :] >= 1, shifted_one, 0.0)
    shifted_two = jnp.where(position[None, :] >= 2, shifted_two, 0.0)
    return (
        taps[2][:, None] * values + taps[1][:, None] * shifted_one + taps[0][:, None] * shifted_two
    )


def ring_plan(sizes, ring):
    free = {"up": 0.0, "down": 0.0, "y": 0.0, "d": 0.0}
    rate = {"up": 46.0, "down": 46.0, "y": 46.0, "d": 330.0}
    waiting = []
    for array in range(len(sizes)):
        for chunk in range(4):
            waiting.append((0.0, array, chunk, 0, 0, None))
    order = []
    pending = []

    def push(ready, send, link, needs):
        pending.append((ready, send, link, needs))

    def ahead(ready, array, chunk, pair, hop, needs):
        link = "up" if chunk % 2 == 0 else "down"
        if hop < ring - 1:
            push(ready, (array, chunk, pair, hop, "z"), link, needs)
        if chunk < 2 and pair == 0 and hop == 0:
            push(ready, (array, chunk, pair, hop, "y"), "y", needs)
        if chunk >= 2 and pair == 0:
            push(ready, (array, chunk, pair, hop, "y"), "y", needs)
        if needs is not None:
            push(ready, (array, chunk, pair, hop, "d"), "d", needs)

    for _, array, chunk, pair, hop, needs in waiting:
        ahead(0.0, array, chunk, pair, hop, needs)
    while pending:
        best = min(
            range(len(pending)),
            key=lambda i: (
                max(pending[i][0], free[pending[i][2]]),
                pending[i][1][0],
                pending[i][0],
                i,
            ),
        )
        ready, send, link, needs = pending.pop(best)
        begin = max(ready, free[link])
        end = begin + sizes[send[0]] / rate[link] / 1e3
        free[link] = end
        order.append((begin, ready, send, needs))
        array, chunk, pair, hop, kind = send
        if kind == "z":
            ahead(end + 2.0, array, chunk, pair, hop + 1, send)
        elif kind == "y":
            if chunk < 2:
                ahead(end + 2.0, array, chunk, 1, 0, send)
            else:
                push(end + 2.0, (array, chunk, 1, hop, "d"), "d", send)
    order.sort(key=lambda item: item[1])
    return [(send, needs) for _, _, send, needs in order]


def gather_kernel(plan, count, groups, shards, *refs):
    own, (own_rows, own_scales) = refs[:count], refs[count : count + 2]
    outs = refs[count + 2 : 2 * count + 2]
    out_rows, out_scales = refs[2 * count + 2 : 2 * count + 4]
    send_sem, recv_sem, local_sem, small_send, small_recv = refs[2 * count + 4 :]
    ring = shards // 2
    place = lax.axis_index("fs")
    core = lax.axis_index("rep")
    group = lax.axis_index("tp")
    z, y = place // 2, place % 2
    up = {"fs": lax.rem(z + 1, ring) * 2 + y}
    down = {"fs": lax.rem(z + ring - 1, ring) * 2 + y}
    across = {"fs": z * 2 + (1 - y)}
    twin = {"rep": 1 - core}

    barrier = pltpu.get_barrier_semaphore()
    others = [{"fs": lax.rem(place + step, shards)} for step in range(1, shards)]
    others += [{"tp": lax.rem(group + step, groups)} for step in range(1, groups)]
    others += [twin]
    for other in others:
        pl.semaphore_signal(barrier, inc=1, device_id=other, device_id_type=MESH)
    pl.semaphore_wait(barrier, len(others))

    small = []
    for step in range(1, groups):
        small.append(
            pltpu.make_async_remote_copy(
                own_rows, out_rows.at[group], small_send.at[step - 1], small_recv.at[step - 1],
                device_id={"tp": lax.rem(group + step, groups)}, device_id_type=MESH,
            )
        )
    for step in range(1, shards):
        index = groups - 1 + step - 1
        small.append(
            pltpu.make_async_remote_copy(
                own_scales, out_scales.at[place], small_send.at[index], small_recv.at[index],
                device_id={"fs": lax.rem(place + step, shards)}, device_id_type=MESH,
            )
        )
    for copy in small:
        copy.start()

    copies = {}
    for number, (send, _) in enumerate(plan):
        array, chunk, pair, hop, kind = send
        step = hop if chunk % 2 == 0 else ring - hop
        owner = lax.rem(z + ring - step, ring) * 2 + (y if pair == 0 else 1 - y)
        slot = outs[array].at[owner, core, chunk]
        source = own[array].at[core, chunk] if (hop == 0 and pair == 0) else slot
        target = {"z": up if chunk % 2 == 0 else down, "y": across, "d": twin}[kind]
        copies[send] = pltpu.make_async_remote_copy(
            source, slot, send_sem.at[number], recv_sem.at[number],
            device_id=target, device_id_type=MESH,
        )

    local = [
        pltpu.make_async_copy(own[array], outs[array].at[place], local_sem.at[array])
        for array in range(count)
    ]
    local.append(pltpu.make_async_copy(own_rows, out_rows.at[group], local_sem.at[count]))
    local.append(pltpu.make_async_copy(own_scales, out_scales.at[place], local_sem.at[count + 1]))

    arrived = set()
    started_local = False
    for send, needs in plan:
        if needs is not None and needs not in arrived:
            if not started_local:
                started_local = True
                for copy in local:
                    copy.start()
            copies[needs].wait_recv()
            arrived.add(needs)
        copies[send].start()
    for send, _ in plan:
        copies[send].wait_send()
        if send not in arrived:
            copies[send].wait_recv()
    for copy in small:
        copy.wait()
    for copy in local:
        copy.wait()


def gather_all(arrays, rows, scales, groups, shards, reps):
    count = len(arrays)
    own = [a.reshape(reps, 4, a.shape[0] // (4 * reps), a.shape[1]) for a in arrays]
    sizes = [a.size // (4 * reps) * a.dtype.itemsize for a in arrays]
    plan = ring_plan(sizes, shards // 2)
    small = groups - 1 + shards - 1
    result = pl.pallas_call(
        functools.partial(gather_kernel, plan, count, groups, shards),
        out_shape=[jax.ShapeDtypeStruct((shards,) + a.shape, a.dtype) for a in own]
        + [
            jax.ShapeDtypeStruct((groups,) + rows.shape, rows.dtype),
            jax.ShapeDtypeStruct((shards,) + scales.shape, scales.dtype),
        ],
        in_specs=[pl.BlockSpec(memory_space=pl.ANY)] * (count + 2),
        out_specs=[pl.BlockSpec(memory_space=pl.ANY)] * (count + 2),
        scratch_shapes=[
            pltpu.SemaphoreType.DMA((len(plan),)),
            pltpu.SemaphoreType.DMA((len(plan),)),
            pltpu.SemaphoreType.DMA((count + 2,)),
            pltpu.SemaphoreType.DMA((small,)),
            pltpu.SemaphoreType.DMA((small,)),
        ],
        compiler_params=pltpu.CompilerParams(collective_id=0, has_side_effects=True),
        name="gather_all",
    )(*own, rows, scales)
    whole = [g.reshape((shards,) + a.shape) for g, a in zip(result, arrays)]
    return whole, result[count], result[count + 1]


def layer_kernel(
    channels, length,
    own_res, mixer_gain, mix_scales, taps, own_gain, channel_gain, gate_scale, up_scale, own_scales,
    *refs,
):
    raw, out_ref, refs = refs[:7], refs[7], refs[8:]
    bufs, refs = refs[:5], refs[5:]
    others, refs = refs[:5], refs[5:]
    stages, refs = refs[:7], refs[7:]
    (res, scales, gains, mixes, after, normed, gate_buf, hidden, outgoing, from_x, to_z, from_z,
     raw_sem, z_send, z_recv, y_send, y_recv, t_send, t_recv, mx_send, mx_recv, mt_send, mt_recv,
     r_send, r_recv, s_send, s_recv, m_send, m_recv, px_send, px_recv, pz_send, pz_recv) = refs
    proj_buf, mout_buf, gate_w, up_w, down_w = bufs
    shards = gate_w.shape[0]
    place = lax.axis_index("fs")
    core = lax.axis_index("rep")
    group = lax.axis_index("tp")
    tokens, own_width = own_res.shape
    features = 2 * own_width
    block = mout_buf.shape[-1]
    per_group = shards // 2
    depth = shards // 2
    width = gate_w.shape[-1]
    narrow = mixes.shape[-1]
    all_tokens = 2 * tokens

    z, y = place // 2, place % 2
    side = z % 2
    part_of = ((z + 1) // 2) % 2
    high = (z * 2 + y) // per_group
    pair = z + 1 - 2 * side
    inner = part_of == 1
    outer = part_of == 0
    opposite = 1 - z // 2
    levels = [z, pair, 1 + opposite, (depth - 1) * opposite]
    twin = {"rep": 1 - core}
    across = {"fs": z * 2 + 1 - y}
    beside = {"tp": 1 - group}
    mate = {"fs": pair * 2 + y}
    corner = {"fs": pair * 2 + y, "tp": 1 - group}

    def remote(source, target, send, recv, device):
        return pltpu.make_async_remote_copy(
            source, target, send, recv, device_id=device, device_id_type=MESH
        )

    def spot(array, owner, half):
        if array == 1:
            return mout_buf.at[owner, group, half]
        if array >= 4:
            return down_w.at[owner, half, array - 4]
        return bufs[array].at[owner, half]

    def owner_of(r, far):
        return levels[r] * 2 + (1 - y if far else y)

    def z_copy(array, way):
        target = spot(array, place, core)
        if array == 1 or way == 2:
            source = target
        else:
            source = others[array - 1 if array else 0]
        level = (None, pair, depth - 1 - z, depth - 1 - pair)[way]
        kind = 0 if way == 1 else 2 - part_of
        return remote(
            source, target, z_send.at[array, way - 1], z_recv.at[array, kind],
            {"fs": level * 2 + y},
        )

    def z_wait(array, r):
        target = spot(array, owner_of(r, False), core)
        remote(
            target, target, z_send.at[array, r - 1], z_recv.at[array, r - 1], across
        ).wait_recv()

    def y_copy(array, r):
        target = spot(array, owner_of(r, False), core)
        return remote(target, target, y_send.at[array, r], y_recv.at[array, r], across)

    def t_copy(array, r, far):
        target = spot(array, owner_of(r, far), core)
        index = r + 4 * far
        return remote(target, target, t_send.at[array, index], t_recv.at[array, index], twin)

    def mx_copy(r, far):
        target = spot(1, owner_of(r, far), core)
        index = r + 4 * far
        return remote(target, target, mx_send.at[index], mx_recv.at[index], beside)

    def mt_copy(r, far):
        target = mout_buf.at[owner_of(r, far), 1 - group, core]
        index = r + 4 * far
        return remote(target, target, mt_send.at[index], mt_recv.at[index], twin)

    rows = stages[0].shape[0]
    tall = stages[6].shape[1]
    raw_copies = []
    for i in range(4):
        raw_copies.append([pltpu.make_async_copy(
            raw[i].at[pl.ds(pl.multiple_of(core * rows, rows), rows)], stages[i], raw_sem.at[i])])
    for i in range(4, 6):
        raw_copies.append([pltpu.make_async_copy(
            raw[i].at[pl.ds(pl.multiple_of(core * rows, rows), rows)], stages[i], raw_sem.at[i])])
    raw_copies.append([
        pltpu.make_async_copy(
            raw[6].at[pl.ds(pl.multiple_of(k * width + core * tall, 16), tall)],
            stages[6].at[k], raw_sem.at[6 + k])
        for k in range(2)
    ])
    for group_of in raw_copies:
        for copy in group_of:
            copy.start()

    barrier = pltpu.get_barrier_semaphore()
    partners = [{"fs": lax.rem(place + step, shards)} for step in range(1, shards)]
    partners += [beside, corner, twin]
    for other in partners:
        pl.semaphore_signal(barrier, inc=1, device_id=other, device_id_type=MESH)
    pl.semaphore_wait(barrier, len(partners))

    scale_copies = [
        remote(own_scales, scales.at[place], s_send.at[step], s_recv.at[step],
               {"fs": lax.rem(place + step, shards)})
        for step in range(1, shards)
    ]
    scale_copies.append(remote(own_gain, gains.at[group], s_send.at[0], s_recv.at[0], beside))
    res_z = remote(own_res, res.at[side, group], r_send.at[0], r_recv.at[0], mate)
    res_x = remote(own_res, res.at[side, group], r_send.at[1], r_recv.at[1], beside)
    passed = res.at[1 - side, group]
    res_d = remote(passed, passed, r_send.at[2], r_recv.at[2], beside)

    def start_z(*pairs):
        for array, r in pairs:
            z_copy(array, r).start()

    def wait_raw(*indices):
        for i in indices:
            for copy in raw_copies[i]:
                copy.wait()

    def both(first, second, size):
        return [
            (first, pl.ds(pl.multiple_of(part_of * size, 128), size)),
            (second, pl.ds(pl.multiple_of((1 - part_of) * size, 128), size)),
        ]

    res_z.start()
    res_x.start()
    wait_raw(0, 1, 2)
    for i in range(3):
        for target, cols in both(proj_buf.at[place, core], others[0], narrow):
            target[:, i * narrow : (i + 1) * narrow] = stages[i][:, cols].astype(jnp.bfloat16)
    start_z((0, 1), (0, 2), (0, 3))
    y_copy(0, 0).start()
    t_copy(0, 0, False).start()
    wait_raw(3)
    mout_buf[place, group, core] = stages[3][...].astype(jnp.bfloat16)
    start_z((1, 1), (1, 2), (1, 3))
    y_copy(1, 0).start()
    mx_copy(0, False).start()
    t_copy(1, 0, False).start()
    for copy in scale_copies:
        copy.start()
    for array in (2, 3):
        wait_raw(array + 2)
        for target, cols in both(bufs[array].at[place, core], others[array - 1], width):
            target[...] = stages[array + 2][:, cols].astype(jnp.bfloat16)
        t_copy(array, 0, False).start()
        if array == 2:
            y_copy(2, 0).start()
            start_z((2, 1))

        @pl.when(inner)
        def _():
            start_z((array, 2), (array, 3))
    wait_raw(6)
    short = tall // 2
    for k, array in ((0, 4), (1, 5)):
        lines = slice(k * short, (k + 1) * short)
        down_w[place, core, k] = stages[6][part_of, lines, :].astype(jnp.bfloat16)
        others[array - 1][...] = stages[6][1 - part_of, lines, :].astype(jnp.bfloat16)
    for array in (4, 5):
        t_copy(array, 0, False).start()
    res[side, group] = own_res[...]
    scales[place] = own_scales[...]
    gains[group] = own_gain[...]

    def take_z(array, r):
        z_wait(array, r)
        y_copy(array, r).start()
        t_copy(array, r, False).start()
        if array == 1:
            mx_copy(r, False).start()

    def take_y(array, r):
        y_copy(array, r).wait_recv()
        t_copy(array, r, True).start()
        if array == 1:
            mx_copy(r, True).start()

    def finish(array):
        for far in (False, True):
            for r in range(4):
                t_copy(array, r, far).wait_recv()

    def scaled(squares, count):
        return lax.rsqrt(squares / count + epsilon)

    def normalize_side(s):
        floats = [res[s, k].astype(jnp.float32) for k in range(2)]
        squares = sum(jnp.sum(row * row, axis=1, keepdims=True) for row in floats)
        factor = scaled(squares, features)
        lines = pl.ds(pl.multiple_of(s * tokens, tokens), tokens)
        for k in range(2):
            cols = slice(k * own_width, (k + 1) * own_width)
            normed[lines, cols] = (
                res[s, k].astype(jnp.float32) * factor * mixer_gain[:, cols]
            ).astype(jnp.bfloat16)

    order = (1, 2, 3)
    take_z(0, 2)
    take_z(1, 2)
    res_z.wait_recv()
    res_d.start()
    for r in (1, 3):
        take_z(0, r)
    for r in (1, 3):
        take_z(1, r)
    y_copy(3, 0).start()
    take_z(2, 2)
    res_x.wait_recv()
    normalize_side(side)
    for r in (0,) + order:
        take_y(0, r)
    for r in (0,) + order:
        take_y(1, r)
    res_d.wait_recv()
    normalize_side(1 - side)
    finish(0)

    own_cols = pl.ds(pl.multiple_of(part_of * narrow, 128), narrow)

    def project(index):
        weight = proj_buf[:, :, :, index * narrow : (index + 1) * narrow].reshape(features, narrow)
        product = jnp.dot(normed[...], weight, preferred_element_type=jnp.float32)
        return product * mix_scales[index : index + 1, own_cols]

    value = project(0)
    u = project(1) * value
    place_in = lax.rem(lax.broadcasted_iota(jnp.int32, u.shape, 0), length)
    one = jnp.where(place_in >= 1, pltpu.roll(u, 1, 0), 0.0)
    two = jnp.where(place_in >= 2, pltpu.roll(u, 2, 0), 0.0)
    conv = taps[2:3, own_cols] * u + taps[1:2, own_cols] * one + taps[0:1, own_cols] * two
    mixes[group, part_of] = (project(2) * conv).astype(jnp.bfloat16)
    mix_slot = mixes.at[group, part_of]
    mix_copies = [
        remote(mix_slot, mix_slot, m_send.at[i], m_recv.at[i], device)
        for i, device in enumerate((mate, beside, corner))
    ]
    for copy in mix_copies:
        copy.start()
    start_z((3, 1))

    @pl.when(outer)
    def _():
        start_z((2, 2), (2, 3))

    start_z((4, 1), (5, 1))

    @pl.when(outer)
    def _():
        start_z((3, 2), (3, 3))

    take_z(2, 1)
    for array in (4, 5):
        y_copy(array, 0).start()
    for far in (False, True):
        for r in range(4):
            mx_copy(r, far).wait_recv()
            mt_copy(r, far).start()
    for copy in scale_copies + mix_copies:
        copy.wait_recv()
    finish(1)
    for far in (False, True):
        for r in range(4):
            mt_copy(r, far).wait_recv()
    total = jnp.zeros((all_tokens, 1), jnp.float32)
    for k in range(2):
        for b in range(2):
            lines = mixes[k, b].astype(jnp.float32)
            total = total + jnp.sum(lines * lines, axis=1, keepdims=True)
    factor = scaled(total, channels)
    for k in range(2):
        for b in range(2):
            cols = slice((2 * k + b) * narrow, (2 * k + b + 1) * narrow)
            hidden[:, cols] = (
                mixes[k, b].astype(jnp.float32) * factor
                * gains[k, 0:1, b * narrow : (b + 1) * narrow]
            ).astype(jnp.bfloat16)
    squares = jnp.zeros((all_tokens, 1), jnp.float32)
    for s in range(shards):
        k, inside = s // per_group, (s % per_group) * block
        part = jnp.dot(
            hidden[:, : 4 * narrow], mout_buf[s].reshape(4 * narrow, block),
            preferred_element_type=jnp.float32,
        ) * scales[s, 0:1, :]
        base = res[:, k, :, inside : inside + block].reshape(all_tokens, block)
        row = (base.astype(jnp.float32) + part).astype(jnp.bfloat16)
        after[s] = row
        row = row.astype(jnp.float32)
        squares = squares + jnp.sum(row * row, axis=1, keepdims=True)
    factor = scaled(squares, features)
    for s in range(shards):
        cols = slice(s * block, (s + 1) * block)
        normed[:, cols] = (
            after[s].astype(jnp.float32) * factor * channel_gain[:, cols]
        ).astype(jnp.bfloat16)

    def tiles(body):
        tile = 256
        whole = width // tile

        @pl.loop(0, whole)
        def _(j):
            body(pl.multiple_of(j * tile, tile), tile)

        if width % tile:
            body(whole * tile, width % tile)

    def multiply(weights, start, size):
        weight = weights[:, :, :, pl.ds(start, size)].reshape(features, size)
        return jnp.dot(normed[...], weight, preferred_element_type=jnp.float32)

    def scale_at(scale, start, size):
        return scale[:, pl.ds(pl.multiple_of(part_of * width + start, 128), size)]

    def gate_tile(start, size):
        gate_buf[:, pl.ds(start, size)] = multiply(gate_w, start, size) * scale_at(
            gate_scale, start, size
        )

    def up_tile(start, size):
        product = multiply(up_w, start, size) * scale_at(up_scale, start, size)
        gate = gate_buf[:, pl.ds(start, size)]
        hidden[:, pl.ds(start, size)] = (
            gate / (1.0 + jnp.exp(-gate)) * product
        ).astype(jnp.bfloat16)

    take_z(3, 2)
    take_z(3, 1)
    take_z(2, 3)
    for r in (0,) + order:
        take_y(2, r)
    finish(2)
    tiles(gate_tile)
    take_z(4, 1)
    take_z(5, 1)
    take_z(3, 3)
    start_z((4, 2), (4, 3), (5, 2), (5, 3))
    for r in (0,) + order:
        take_y(3, r)
    finish(3)
    tiles(up_tile)

    steps = [(r, far) for r in range(4) for far in (False, True)]

    def index_of(k):
        return owner_of(*steps[k])

    def mine(k):
        return (high == group) if k < per_group else (high != group)

    def slot_of(k):
        return lax.rem(index_of(k), per_group)

    def px_copy(k, which):
        who = 1 - side if which == 0 else side
        return remote(
            outgoing.at[k, who], from_x.at[k, who], px_send.at[k, which], px_recv.at[k, which], beside
        )

    def pz_copy(k):
        i = slot_of(k)
        return remote(to_z.at[i], from_z.at[i], pz_send.at[i], pz_recv.at[i], mate)

    def down(k):
        r, far = steps[k]
        for array in (4, 5):
            t_copy(array, r, far).wait_recv()
        s = index_of(k)
        weight = down_w[s].reshape(width, block)
        part = jnp.dot(hidden[...], weight, preferred_element_type=jnp.float32)
        part = (part * scales[s, 1:2, :]).astype(jnp.bfloat16)
        outgoing[k, 0] = part[:tokens]
        outgoing[k, 1] = part[tokens:]

        @pl.when(jnp.logical_not(mine(k)))
        def _():
            px_copy(k, 0).start()
            px_copy(k, 1).start()

    def pass_on(k):
        @pl.when(mine(k))
        def _():
            px_copy(k, 0).wait_recv()
            to_z[slot_of(k)] = (
                outgoing[k, 1 - side].astype(jnp.float32) + from_x[k, 1 - side].astype(jnp.float32)
            ).astype(jnp.bfloat16)
            pz_copy(k).start()

    def close(k):
        i = slot_of(k)
        s = index_of(k)

        @pl.when(mine(k))
        def _():
            px_copy(k, 1).wait_recv()
            pz_copy(k).wait_recv()
            lines = pl.ds(pl.multiple_of(side * tokens, tokens), tokens)
            total = outgoing[k, side].astype(jnp.float32) + from_x[k, side].astype(jnp.float32)
            total = total + from_z[i].astype(jnp.float32)
            out_ref[:, pl.ds(pl.multiple_of(i * block, block), block)] = (
                after[s, lines, :].astype(jnp.float32) + total
            ).astype(jnp.bfloat16)

    def take_all(take, r):
        for array in (4, 5):
            take(array, r)

    down(0)
    take_all(take_y, 0)
    down(1)
    down(2)
    take_all(take_y, 1)
    down(3)
    take_all(take_z, 2)
    down(4)
    pass_on(0)
    pass_on(1)
    take_all(take_y, 2)
    down(5)
    pass_on(2)
    pass_on(3)
    take_all(take_z, 3)
    pass_on(4)
    down(6)
    pass_on(5)
    take_all(take_y, 3)
    down(7)
    for k in range(per_group):
        close(k)
    pass_on(6)
    pass_on(7)
    for k in range(per_group, shards):
        close(k)

    for array in range(6):
        for r in range(4):
            if r:
                z_copy(array, r).wait_send()
            y_copy(array, r).wait_send()
            for far in (False, True):
                t_copy(array, r, far).wait_send()
    for r in range(4):
        for far in (False, True):
            mx_copy(r, far).wait_send()
            mt_copy(r, far).wait_send()
    for copy in scale_copies + mix_copies + [res_z, res_x, res_d]:
        copy.wait_send()
    for k in range(len(steps)):
        @pl.when(mine(k))
        def _():
            pz_copy(k).wait_send()

        @pl.when(jnp.logical_not(mine(k)))
        def _():
            px_copy(k, 0).wait_send()
            px_copy(k, 1).wait_send()


def fused(
    shards, residual, mixer_gain, mix_scales, taps, conv_gain, channel_gain,
    gate_scale, up_scale, scales, raw,
):
    tokens, own_width = residual.shape
    features = 2 * own_width
    short = jnp.bfloat16
    in_rows, mix_width = raw[0].shape
    rows, narrow = in_rows // 2, mix_width // 2
    ff = gate_scale.shape[1]
    width = ff // 2
    out_rows, block = raw[3].shape
    channels = 2 * out_rows
    tall = width // 2
    steps = shards
    vmem = pl.BlockSpec(memory_space=pltpu.VMEM)
    dma = pltpu.SemaphoreType.DMA
    return pl.pallas_call(
        functools.partial(layer_kernel, channels, LEN),
        out_shape=jax.ShapeDtypeStruct((tokens, own_width), short),
        in_specs=[vmem] * 9 + [pl.BlockSpec(memory_space=pl.ANY)] * 7,
        out_specs=vmem,
        scratch_shapes=[
            pltpu.VMEM((shards, 2, rows, 3 * narrow), short),
            pltpu.VMEM((shards, 2, 2, out_rows // 2, block), short),
            pltpu.VMEM((shards, 2, rows, width), short),
            pltpu.VMEM((shards, 2, rows, width), short),
            pltpu.VMEM((shards, 2, 2, tall // 2, block), short),
            pltpu.VMEM((rows, 3 * narrow), short),
            pltpu.VMEM((rows, width), short),
            pltpu.VMEM((rows, width), short),
            pltpu.VMEM((tall // 2, block), short),
            pltpu.VMEM((tall // 2, block), short),
        ]
        + [pltpu.VMEM((rows, mix_width), jnp.float32)] * 3
        + [
            pltpu.VMEM((out_rows // 2, block), jnp.float32),
            pltpu.VMEM((rows, ff), jnp.float32),
            pltpu.VMEM((rows, ff), jnp.float32),
            pltpu.VMEM((2, tall, block), jnp.float32),
            pltpu.VMEM((2, 2, tokens, own_width), short),
            pltpu.VMEM((shards,) + scales.shape, jnp.float32),
            pltpu.VMEM((2,) + conv_gain.shape, jnp.float32),
            pltpu.VMEM((2, 2, 2 * tokens, narrow), short),
            pltpu.VMEM((shards, 2 * tokens, block), short),
            pltpu.VMEM((2 * tokens, features), short),
            pltpu.VMEM((2 * tokens, width), jnp.float32),
            pltpu.VMEM((2 * tokens, width), short),
            pltpu.VMEM((steps, 2, tokens, block), short),
            pltpu.VMEM((steps, 2, tokens, block), short),
            pltpu.VMEM((steps // 2, tokens, block), short),
            pltpu.VMEM((steps // 2, tokens, block), short),
            dma((8,)),
            dma((6, 3)),
            dma((6, 3)),
            dma((6, 4)),
            dma((6, 4)),
            dma((6, 8)),
            dma((6, 8)),
            dma((8,)),
            dma((8,)),
            dma((8,)),
            dma((8,)),
            dma((3,)),
            dma((3,)),
            dma((shards,)),
            dma((shards,)),
            dma((3,)),
            dma((3,)),
            dma((steps, 2)),
            dma((steps, 2)),
            dma((steps // 2,)),
            dma((steps // 2,)),
        ],
        compiler_params=pltpu.CompilerParams(
            collective_id=1, has_side_effects=True, vmem_limit_bytes=60 * 1024 * 1024
        ),
        name="layer",
    )(
        residual, mixer_gain, mix_scales, taps, conv_gain, channel_gain, gate_scale, up_scale,
        scales, *raw,
    )


def local(
    reps,
    shards,
    groups,
    residual,
    mixer_gain,
    value_weight,
    value_scale,
    input_gate_weight,
    input_gate_scale,
    output_gate_weight,
    output_gate_scale,
    conv_taps,
    conv_gain,
    mixer_out_weight,
    mixer_out_scale,
    channel_gain,
    gate_weight,
    gate_scale,
    up_weight,
    up_scale,
    down_weight,
    down_scale,
):
    own_rows, tokens = residual.shape
    width = value_weight.shape[1]
    channels = width * groups
    features = own_rows * groups
    short = jnp.bfloat16
    block, ff = mixer_out_weight.shape[1], gate_weight.shape[1]
    in_rows, out_rows = value_weight.shape[0], mixer_out_weight.shape[0]
    if (
        reps == 2 and groups == 2 and shards == 8 and tokens % LEN == 0
        and block % 128 == 0 and width % 256 == 0 and ff % 256 == 0 and ff % 128 == 0
        and in_rows % 32 == 0 and out_rows == width and own_rows == block * shards // 2
    ):
        pad = jnp.zeros((7, width), jnp.float32)
        result = fused(
            shards, residual.T, mixer_gain[None],
            jnp.stack([value_scale, input_gate_scale, output_gate_scale]), conv_taps,
            jnp.concatenate([conv_gain[None], pad]), channel_gain[None], gate_scale[None], up_scale[None],
            jnp.pad(jnp.stack([mixer_out_scale, down_scale]), ((0, 6), (0, 0))),
            [value_weight, input_gate_weight, output_gate_weight, mixer_out_weight,
             gate_weight, up_weight, down_weight],
        )
        return result.T
    projections = jnp.concatenate(
        [value_weight.astype(short), input_gate_weight.astype(short), output_gate_weight.astype(short)],
        axis=1,
    )
    arrays = [
        projections,
        mixer_out_weight.astype(short),
        gate_weight.astype(short),
        up_weight.astype(short),
        down_weight.astype(short),
    ]
    scales = jnp.stack([mixer_out_scale, down_scale])
    (proj_all, out_all, gate_all, up_all, down_all), rows_all, scales_all = gather_all(
        arrays, residual, scales, groups, shards, reps
    )
    whole = rows_all.reshape(features, tokens)
    out_scale = scales_all[:, 0].reshape(features)
    down_scale_full = scales_all[:, 1].reshape(features)

    normed = normalize(whole, mixer_gain)
    projected = contract(proj_all.reshape(features, 3 * width), normed)
    value = projected[:width] * value_scale[:, None]
    in_gate = projected[width : 2 * width] * input_gate_scale[:, None]
    out_gate = projected[2 * width :] * output_gate_scale[:, None]
    mixed = out_gate * causal_conv(in_gate * value, conv_taps, LEN)
    squares = lax.psum(jnp.sum(mixed * mixed, axis=0), "tp")
    conv_normed = (
        mixed * lax.rsqrt(squares / channels + epsilon)[None, :] * conv_gain[:, None]
    ).astype(short)
    part = lax.dot_general(
        out_all, conv_normed, (((1,), (0,)), ((), ())), preferred_element_type=jnp.float32
    ).reshape(features, tokens)
    rounded = (part * out_scale[:, None]).astype(short)
    parts = lax.all_gather(rounded, "tp", axis=0)
    total = jnp.sum(parts.astype(jnp.float32), axis=0)
    after_whole = (whole.astype(jnp.float32) + total).astype(short)
    after_own = lax.dynamic_slice_in_dim(
        after_whole, lax.axis_index("tp") * own_rows, own_rows, 0
    )
    normed_two = normalize(after_whole, channel_gain)
    gate = contract(gate_all.reshape(features, -1), normed_two)
    upper = contract(up_all.reshape(features, -1), normed_two)
    hidden = (jax.nn.silu(gate * gate_scale[:, None]) * (upper * up_scale[:, None])).astype(short)
    down = lax.dot_general(
        down_all, hidden, (((1,), (0,)), ((), ())), preferred_element_type=jnp.float32
    ).reshape(features, tokens)
    total_two = lax.psum_scatter(
        (down * down_scale_full[:, None]).astype(short),
        "tp",
        scatter_dimension=0,
        tiled=True,
    ).astype(jnp.float32)
    return (after_own.astype(jnp.float32) + total_two).astype(short)


def solution(mesh):
    placed = (
        P("tp", ("rep", "fs")),
        P(),
        P("fs", "tp"),
        P("tp"),
        P("fs", "tp"),
        P("tp"),
        P("fs", "tp"),
        P("tp"),
        P(None, "tp"),
        P("tp"),
        P("tp", "fs"),
        P("fs"),
        P(),
        P("fs", "tp"),
        P("tp"),
        P("fs", "tp"),
        P("tp"),
        P("tp", "fs"),
        P("fs"),
    )
    sizes = mesh.shape["rep"], mesh.shape["fs"], mesh.shape["tp"]
    return jax.shard_map(
        functools.partial(local, *sizes),
        mesh=mesh,
        in_specs=placed,
        out_specs=P("tp", ("rep", "fs")),
        check_vma=False,
    )
```

profile of v0, /device:TPU:0, one launch (start us, length us, event | category | flops | bytes accessed | tf_op | source)
XLA Modules:
  0.0 172.5 jit_solution(3874562449359922394)
XLA Ops:
  0.0 1.3 pad_maximum_fusion.mix_scales
  1.3 1.3 concatenate.3.own_gain
  2.6 1.3 select_maximum_fusion.own_scales
  3.9 1.3 broadcast_in_dim.19.gate_scale
  5.2 1.3 broadcast_in_dim.20.up_scale
  6.5 2.0 %copy.20 = bf16[1024,256]{0,1:T(8,128)(2,1)} copy(bf16[1024,256]{1,0:T(8,128)(2,1)} %param.19) | data formatting | bytes 1048576 | tf_op args[0]
  8.5 161.9 %layer.1 = bf16[256,1024]{1,0:T(8,128)(2,1)} custom-call(bf16[256,1024]{1,0:T(8,128)(2,1)} %bitcast.11, f32[1,2048]{1,0:T(1,128)} %bitcast.12, f32[3,256]{1,0:T(4,128)} %pad_maximum_fusion.mix_scales, f32[3,256]{1,0:T(4,128)} %taps.1, f32[8,256]{1,0:T(8,128)} %concatenate.3.own_gain, f32[1,2048]{1,0:T(1,128)} %bitcast.13, ...), custom_call_target="tpu_custom_call" | custom-call | tf_op jit(solution)/shard_map/layer/pallas_call | solution.py:702
  170.4 2.0 %copy.21 = bf16[1024,256]{1,0:T(8,128)(2,1)} copy(bf16[1024,256]{0,1:T(8,128)(2,1)} %bitcast.10) | data formatting | bytes 1048576 | tf_op jit(solution)/shard_map/transpose | solution.py:814
where the time goes:
time: 175 us; the launch traced here: 172 us
  Pallas kernels  162 us (93%)
  local copies, waits for them, and re-layouts  7.97 us (5%)
  other arithmetic  2.61 us (1%)
    pallas_call x1, Pallas kernels, fused(): pl.pallas_call(functools.partial(layer_kernel, channels, LEN), out_shape=...  162 us

commit v1 on v0

--- a/solution.py
+++ b/solution.py
@@ -204,22 +204,25 @@
 
 def layer_kernel(
     channels, length,
-    own_res, mixer_gain, mix_scales, taps, own_gain, channel_gain, gate_scale, up_scale, own_scales,
+    residual, mixer_gain, value_scale, input_scale, output_scale, taps, conv_gain, channel_gain,
+    gate_scale, up_scale, out_scale, down_scale,
     *refs,
 ):
     raw, out_ref, refs = refs[:7], refs[7], refs[8:]
     bufs, refs = refs[:5], refs[5:]
     others, refs = refs[:5], refs[5:]
     stages, refs = refs[:7], refs[7:]
-    (res, scales, gains, mixes, after, normed, gate_buf, hidden, outgoing, from_x, to_z, from_z,
+    (own_res, own_scales, res, scales, gains, mixes, after, normed, gate_buf, hidden, outgoing, from_x, to_z, from_z, to_x, whole_z,
      raw_sem, z_send, z_recv, y_send, y_recv, t_send, t_recv, mx_send, mx_recv, mt_send, mt_recv,
-     r_send, r_recv, s_send, s_recv, m_send, m_recv, px_send, px_recv, pz_send, pz_recv) = refs
+     r_send, r_recv, s_send, s_recv, m_send, m_recv, px_send, px_recv, pz_send, pz_recv,
+     zz_send, zz_recv) = refs
     proj_buf, mout_buf, gate_w, up_w, down_w = bufs
     shards = gate_w.shape[0]
     place = lax.axis_index("fs")
     core = lax.axis_index("rep")
     group = lax.axis_index("tp")
-    tokens, own_width = own_res.shape
+    own_width, tokens = residual.shape
+    mix_scales = (value_scale, input_scale, output_scale)
     features = 2 * own_width
     block = mout_buf.shape[-1]
     per_group = shards // 2
@@ -259,13 +262,13 @@
         return levels[r] * 2 + (1 - y if far else y)
 
     def z_copy(array, way):
-        target = spot(array, place, core)
-        if array == 1 or way == 2:
+        target = spot(array, pair * 2 + y if way == 4 else place, core)
+        if array == 1 or way in (2, 4):
             source = target
         else:
             source = others[array - 1 if array else 0]
-        level = (None, pair, depth - 1 - z, depth - 1 - pair)[way]
-        kind = 0 if way == 1 else 2 - part_of
+        level = (None, pair, depth - 1 - z, depth - 1 - pair, depth - 1 - z)[way]
+        kind = (None, 0, 2 - part_of, 2 - part_of, 2)[way]
         return remote(
             source, target, z_send.at[array, way - 1], z_recv.at[array, kind],
             {"fs": level * 2 + y},
@@ -315,6 +318,12 @@
         for copy in group_of:
             copy.start()
 
+    for first in range(0, own_width, tokens):
+        own_res[:, first : first + tokens] = residual[first : first + tokens, :].T
+    own_scales[...] = jnp.concatenate(
+        [out_scale[...], down_scale[...], conv_gain[...], jnp.zeros((5, block), jnp.float32)], axis=0
+    )
+
     barrier = pltpu.get_barrier_semaphore()
     partners = [{"fs": lax.rem(place + step, shards)} for step in range(1, shards)]
     partners += [beside, corner, twin]
@@ -327,7 +336,7 @@
                {"fs": lax.rem(place + step, shards)})
         for step in range(1, shards)
     ]
-    scale_copies.append(remote(own_gain, gains.at[group], s_send.at[0], s_recv.at[0], beside))
+    scale_copies.append(remote(own_scales, gains.at[group], s_send.at[0], s_recv.at[0], beside))
     res_z = remote(own_res, res.at[side, group], r_send.at[0], r_recv.at[0], mate)
     res_x = remote(own_res, res.at[side, group], r_send.at[1], r_recv.at[1], beside)
     passed = res.at[1 - side, group]
@@ -336,6 +345,18 @@
     def start_z(*pairs):
         for array, r in pairs:
             z_copy(array, r).start()
+
+    def start_inner(*pairs):
+        @pl.when(inner)
+        def _():
+            for array, way in pairs:
+                z_copy(array, way).start()
+
+    def start_outer(*pairs):
+        @pl.when(outer)
+        def _():
+            for array, way in pairs:
+                z_copy(array, way).start()
 
     def wait_raw(*indices):
         for i in indices:
@@ -373,10 +394,7 @@
         if array == 2:
             y_copy(2, 0).start()
             start_z((2, 1))
-
-        @pl.when(inner)
-        def _():
-            start_z((array, 2), (array, 3))
+            start_inner((2, 2))
     wait_raw(6)
     short = tall // 2
     for k, array in ((0, 4), (1, 5)):
@@ -387,10 +405,12 @@
         t_copy(array, 0, False).start()
     res[side, group] = own_res[...]
     scales[place] = own_scales[...]
-    gains[group] = own_gain[...]
+    gains[group] = own_scales[...]
 
     def take_z(array, r):
         z_wait(array, r)
+        if r == 1 and array >= 2:
+            start_inner((array, 4))
         y_copy(array, r).start()
         t_copy(array, r, False).start()
         if array == 1:
@@ -401,6 +421,24 @@
         t_copy(array, r, True).start()
         if array == 1:
             mx_copy(r, True).start()
+
+    def run(items):
+        for kind, array, r in items:
+            if kind == "s":
+                z_copy(array, r).start()
+            elif kind == "o":
+                y_copy(array, r).start()
+            else:
+                (take_z if kind == "z" else take_y)(array, r)
+
+    def each(outer_items, inner_items):
+        @pl.when(outer)
+        def _():
+            run(outer_items)
+
+        @pl.when(inner)
+        def _():
+            run(inner_items)
 
     def finish(array):
         for far in (False, True):
@@ -426,18 +464,16 @@
     take_z(1, 2)
     res_z.wait_recv()
     res_d.start()
-    for r in (1, 3):
-        take_z(0, r)
-    for r in (1, 3):
-        take_z(1, r)
+    start_inner((2, 3))
+    start_outer((2, 2))
+    take_z(0, 1)
+    take_z(0, 3)
     y_copy(3, 0).start()
-    take_z(2, 2)
+    y_copy(4, 0).start()
     res_x.wait_recv()
     normalize_side(side)
-    for r in (0,) + order:
+    for r in (0, 2, 1, 3):
         take_y(0, r)
-    for r in (0,) + order:
-        take_y(1, r)
     res_d.wait_recv()
     normalize_side(1 - side)
     finish(0)
@@ -447,7 +483,7 @@
     def project(index):
         weight = proj_buf[:, :, :, index * narrow : (index + 1) * narrow].reshape(features, narrow)
         product = jnp.dot(normed[...], weight, preferred_element_type=jnp.float32)
-        return product * mix_scales[index : index + 1, own_cols]
+        return product * mix_scales[index][:, own_cols]
 
     value = project(0)
     u = project(1) * value
@@ -464,20 +500,16 @@
     for copy in mix_copies:
         copy.start()
     start_z((3, 1))
-
-    @pl.when(outer)
-    def _():
-        start_z((2, 2), (2, 3))
-
+    start_outer((3, 2))
     start_z((4, 1), (5, 1))
-
-    @pl.when(outer)
-    def _():
-        start_z((3, 2), (3, 3))
-
-    take_z(2, 1)
-    for array in (4, 5):
-        y_copy(array, 0).start()
+    each(
+        [("z", 1, 3), ("z", 2, 2), ("z", 1, 1), ("z", 2, 3), ("z", 2, 1)],
+        [("z", 1, 1), ("z", 1, 3), ("z", 2, 2), ("z", 2, 1)],
+    )
+    start_inner((3, 2), (3, 3))
+    y_copy(5, 0).start()
+    for r in (0, 2, 1, 3):
+        take_y(1, r)
     for far in (False, True):
         for r in range(4):
             mx_copy(r, far).wait_recv()
@@ -499,7 +531,7 @@
             cols = slice((2 * k + b) * narrow, (2 * k + b + 1) * narrow)
             hidden[:, cols] = (
                 mixes[k, b].astype(jnp.float32) * factor
-                * gains[k, 0:1, b * narrow : (b + 1) * narrow]
+                * gains[k, 2:3, b * narrow : (b + 1) * narrow]
             ).astype(jnp.bfloat16)
     squares = jnp.zeros((all_tokens, 1), jnp.float32)
     for s in range(shards):
@@ -536,7 +568,9 @@
         return jnp.dot(normed[...], weight, preferred_element_type=jnp.float32)
 
     def scale_at(scale, start, size):
-        return scale[:, pl.ds(pl.multiple_of(part_of * width + start, 128), size)]
+        first = part_of * (width // 128) + start // 128
+        lines = [scale[pl.ds(first + i, 1), :] for i in range(size // 128)]
+        return jnp.concatenate(lines, axis=1)
 
     def gate_tile(start, size):
         gate_buf[:, pl.ds(start, size)] = multiply(gate_w, start, size) * scale_at(
@@ -550,19 +584,18 @@
             gate / (1.0 + jnp.exp(-gate)) * product
         ).astype(jnp.bfloat16)
 
-    take_z(3, 2)
-    take_z(3, 1)
-    take_z(2, 3)
+    each([], [("z", 2, 3), ("z", 3, 1)])
+    start_inner((4, 2), (5, 2))
     for r in (0,) + order:
         take_y(2, r)
     finish(2)
     tiles(gate_tile)
-    take_z(4, 1)
-    take_z(5, 1)
-    take_z(3, 3)
-    start_z((4, 2), (4, 3), (5, 2), (5, 3))
-    for r in (0,) + order:
-        take_y(3, r)
+    each(
+        [("z", 3, 2), ("z", 3, 3), ("s", 4, 2), ("s", 5, 2), ("z", 3, 1), ("z", 4, 1), ("z", 5, 1), ("y", 3, 0),
+         ("y", 3, 2), ("y", 3, 3), ("y", 3, 1)],
+        [("z", 3, 2), ("z", 3, 3), ("s", 4, 3), ("s", 5, 3), ("z", 4, 1), ("z", 5, 1), ("y", 3, 0), ("y", 3, 1),
+         ("y", 3, 2), ("z", 4, 2), ("z", 5, 2), ("y", 3, 3)],
+    )
     finish(3)
     tiles(up_tile)
 
@@ -580,12 +613,16 @@
     def px_copy(k, which):
         who = 1 - side if which == 0 else side
         return remote(
-            outgoing.at[k, who], from_x.at[k, who], px_send.at[k, which], px_recv.at[k, which], beside
+            to_x.at[k] if k % 2 else outgoing.at[k, who], from_x.at[k, who], px_send.at[k, which], px_recv.at[k, which], beside
         )
 
     def pz_copy(k):
         i = slot_of(k)
         return remote(to_z.at[i], from_z.at[i], pz_send.at[i], pz_recv.at[i], mate)
+
+    def zz_copy(k):
+        s = index_of(k)
+        return remote(outgoing.at[k, 1 - side], whole_z.at[s], zz_send.at[s], zz_recv.at[s], mate)
 
     def down(k):
         r, far = steps[k]
@@ -598,12 +635,28 @@
         outgoing[k, 0] = part[:tokens]
         outgoing[k, 1] = part[tokens:]
 
+        if k % 2:
+            zz_copy(k).start()
+            return
+
         @pl.when(jnp.logical_not(mine(k)))
         def _():
             px_copy(k, 0).start()
             px_copy(k, 1).start()
 
     def pass_on(k):
+        if k % 2:
+            zz_copy(k).wait_recv()
+
+            @pl.when(jnp.logical_not(mine(k)))
+            def _():
+                to_x[k] = (
+                    outgoing[k, side].astype(jnp.float32) + whole_z[index_of(k)].astype(jnp.float32)
+                ).astype(jnp.bfloat16)
+                px_copy(k, 1).start()
+
+            return
+
         @pl.when(mine(k))
         def _():
             px_copy(k, 0).wait_recv()
@@ -619,10 +672,11 @@
         @pl.when(mine(k))
         def _():
             px_copy(k, 1).wait_recv()
-            pz_copy(k).wait_recv()
+            if k % 2 == 0:
+                pz_copy(k).wait_recv()
             lines = pl.ds(pl.multiple_of(side * tokens, tokens), tokens)
             total = outgoing[k, side].astype(jnp.float32) + from_x[k, side].astype(jnp.float32)
-            total = total + from_z[i].astype(jnp.float32)
+            total = total + (whole_z[s] if k % 2 else from_z[i]).astype(jnp.float32)
             out_ref[:, pl.ds(pl.multiple_of(i * block, block), block)] = (
                 after[s, lines, :].astype(jnp.float32) + total
             ).astype(jnp.bfloat16)
@@ -631,36 +685,43 @@
         for array in (4, 5):
             take(array, r)
 
+    each([("z", 4, 2), ("z", 5, 2)], [])
     down(0)
     take_all(take_y, 0)
     down(1)
     down(2)
     take_all(take_y, 1)
     down(3)
-    take_all(take_z, 2)
     down(4)
-    pass_on(0)
+    take_all(take_z, 3)
     pass_on(1)
     take_all(take_y, 2)
     down(5)
-    pass_on(2)
+    down(6)
     pass_on(3)
-    take_all(take_z, 3)
+    pass_on(0)
     pass_on(4)
-    down(6)
     pass_on(5)
     take_all(take_y, 3)
     down(7)
-    for k in range(per_group):
+    pass_on(6)
+    pass_on(2)
+    pass_on(7)
+    for k in range(shards):
         close(k)
-    pass_on(6)
-    pass_on(7)
-    for k in range(per_group, shards):
-        close(k)
+
+    z_copy(0, 3).wait_send()
+    z_copy(1, 3).wait_send()
+
+    @pl.when(inner)
+    def _():
+        for array in range(2, 6):
+            for way in (3, 4):
+                z_copy(array, way).wait_send()
 
     for array in range(6):
         for r in range(4):
-            if r:
+            if r in (1, 2):
                 z_copy(array, r).wait_send()
             y_copy(array, r).wait_send()
             for far in (False, True):
@@ -671,27 +732,28 @@
             mt_copy(r, far).wait_send()
     for copy in scale_copies + mix_copies + [res_z, res_x, res_d]:
         copy.wait_send()
-    for k in range(len(steps)):
-        @pl.when(mine(k))
-        def _():
-            pz_copy(k).wait_send()
+    for k in range(shards):
+        if k % 2:
+            zz_copy(k).wait_send()
+        else:
+            pl.when(mine(k))(pz_copy(k).wait_send)
 
         @pl.when(jnp.logical_not(mine(k)))
         def _():
-            px_copy(k, 0).wait_send()
+            if k % 2 == 0:
+                px_copy(k, 0).wait_send()
             px_copy(k, 1).wait_send()
 
 
 def fused(
-    shards, residual, mixer_gain, mix_scales, taps, conv_gain, channel_gain,
-    gate_scale, up_scale, scales, raw,
+    shards, residual, small, raw,
 ):
-    tokens, own_width = residual.shape
+    own_width, tokens = residual.shape
     features = 2 * own_width
     short = jnp.bfloat16
     in_rows, mix_width = raw[0].shape
     rows, narrow = in_rows // 2, mix_width // 2
-    ff = gate_scale.shape[1]
+    ff = raw[4].shape[1]
     width = ff // 2
     out_rows, block = raw[3].shape
     channels = 2 * out_rows
@@ -702,7 +764,7 @@
     return pl.pallas_call(
         functools.partial(layer_kernel, channels, LEN),
         out_shape=jax.ShapeDtypeStruct((tokens, own_width), short),
-        in_specs=[vmem] * 9 + [pl.BlockSpec(memory_space=pl.ANY)] * 7,
+        in_specs=[vmem] * (1 + len(small)) + [pl.BlockSpec(memory_space=pl.ANY)] * 7,
         out_specs=vmem,
         scratch_shapes=[
             pltpu.VMEM((shards, 2, rows, 3 * narrow), short),
@@ -722,9 +784,11 @@
             pltpu.VMEM((rows, ff), jnp.float32),
             pltpu.VMEM((rows, ff), jnp.float32),
             pltpu.VMEM((2, tall, block), jnp.float32),
+            pltpu.VMEM((tokens, own_width), short),
+            pltpu.VMEM((8, block), jnp.float32),
             pltpu.VMEM((2, 2, tokens, own_width), short),
-            pltpu.VMEM((shards,) + scales.shape, jnp.float32),
-            pltpu.VMEM((2,) + conv_gain.shape, jnp.float32),
+            pltpu.VMEM((shards, 8, block), jnp.float32),
+            pltpu.VMEM((2, 8, block), jnp.float32),
             pltpu.VMEM((2, 2, 2 * tokens, narrow), short),
             pltpu.VMEM((shards, 2 * tokens, block), short),
             pltpu.VMEM((2 * tokens, features), short),
@@ -734,8 +798,10 @@
             pltpu.VMEM((steps, 2, tokens, block), short),
             pltpu.VMEM((steps // 2, tokens, block), short),
             pltpu.VMEM((steps // 2, tokens, block), short),
+            pltpu.VMEM((steps, tokens, block), short),
+            pltpu.VMEM((steps, tokens, block), short),
             dma((8,)),
-            dma((6, 3)),
+            dma((6, 4)),
             dma((6, 3)),
             dma((6, 4)),
             dma((6, 4)),
@@ -755,14 +821,15 @@
             dma((steps, 2)),
             dma((steps // 2,)),
             dma((steps // 2,)),
+            dma((steps,)),
+            dma((steps,)),
         ],
         compiler_params=pltpu.CompilerParams(
             collective_id=1, has_side_effects=True, vmem_limit_bytes=60 * 1024 * 1024
         ),
         name="layer",
     )(
-        residual, mixer_gain, mix_scales, taps, conv_gain, channel_gain, gate_scale, up_scale,
-        scales, *raw,
+        residual, *small, *raw,
     )
 
 
@@ -799,15 +866,14 @@
     in_rows, out_rows = value_weight.shape[0], mixer_out_weight.shape[0]
     if (
         reps == 2 and groups == 2 and shards == 8 and tokens % LEN == 0
-        and block % 128 == 0 and width % 256 == 0 and ff % 256 == 0 and ff % 128 == 0
+        and block % 128 == 0 and width % 256 == 0 and ff % 256 == 0 and block == width
         and in_rows % 32 == 0 and out_rows == width and own_rows == block * shards // 2
     ):
-        pad = jnp.zeros((7, width), jnp.float32)
         result = fused(
-            shards, residual.T, mixer_gain[None],
-            jnp.stack([value_scale, input_gate_scale, output_gate_scale]), conv_taps,
-            jnp.concatenate([conv_gain[None], pad]), channel_gain[None], gate_scale[None], up_scale[None],
-            jnp.pad(jnp.stack([mixer_out_scale, down_scale]), ((0, 6), (0, 0))),
+            shards, residual,
+            [mixer_gain[None], value_scale[None], input_gate_scale[None], output_gate_scale[None],
+             conv_taps, conv_gain[None], channel_gain[None], gate_scale.reshape(-1, 128),
+             up_scale.reshape(-1, 128), mixer_out_scale[None], down_scale[None]],
             [value_weight, input_gate_weight, output_gate_weight, mixer_out_weight,
              gate_weight, up_weight, down_weight],
         )

time: 175 us -> 145 us (0.83); the launches traced: 172 us -> 144 us
  Pallas kernels: 162 us -> 142 us
  local copies, waits for them, and re-layouts: 7.97 us -> 2.04 us
  other arithmetic: 2.61 us -> 0 us
    pallas_call x1, Pallas kernels: 162 us -> 142 us  [fused(): pl.pallas_call(functools.partial(layer_kernel, channels, LEN), out_shape=...]
    broadcast_in_dim x2 -> x0, local copies, waits for them, and re-layouts: 2.62 us -> none  [the longest x1 1.31 us: local(): gate_scale[None]]
    another operation x2 -> x0, other arithmetic: 2.61 us -> none  [the longest x1 1.31 us: local(): jnp.stack([value_scale, input_gate_scale, output_gate_scale])]
    unnamed x1 -> x0, local copies, waits for them, and re-layouts: 2.04 us -> none
where the time goes in v1:
time: 145 us; the launch traced here: 144 us
  Pallas kernels  142 us (98%)
  local copies, waits for them, and re-layouts  2.04 us (1%)
    pallas_call x1, Pallas kernels, fused(): pl.pallas_call(functools.partial(layer_kernel, channels, LEN), out_shape=...  142 us

profile of v1, /device:TPU:0, one launch (start us, length us, event | category | flops | bytes accessed | tf_op | source)
XLA Modules:
  0.0 144.3 jit_solution(5066314439015367284)
XLA Ops:
  0.0 142.2 %layer.1 = bf16[256,1024]{1,0:T(8,128)(2,1)} custom-call(bf16[1024,256]{1,0:T(8,128)(2,1)} %residual.1, f32[1,2048]{1,0:T(1,128)} %bitcast.14, f32[1,256]{1,0:T(1,128)} %bitcast.16, f32[1,256]{1,0:T(1,128)} %bitcast.17, f32[1,256]{1,0:T(1,128)} %bitcast.18, f32[3,256]{1,0:T(4,128)} %taps.1, f32[1,256]{1,0:T(1,128)} %bitcast.19, f32[1,2048]{1,0:T(1,128)} %bitcast.15, ...), custom_call_target="tpu_custom_call" | custom-call | tf_op jit(solution)/shard_map/layer/pallas_call | solution.py:764
  142.2 2.0 %copy.20 = bf16[1024,256]{1,0:T(8,128)(2,1)} copy(bf16[1024,256]{0,1:T(8,128)(2,1)} %bitcast.11) | data formatting | bytes 1048576 | tf_op jit(solution)/shard_map/transpose | solution.py:880

commit v2 on v1

--- a/solution.py
+++ b/solution.py
@@ -210,12 +210,12 @@
 ):
     raw, out_ref, refs = refs[:7], refs[7], refs[8:]
     bufs, refs = refs[:5], refs[5:]
-    others, refs = refs[:5], refs[5:]
+    others, refs = refs[:7], refs[7:]
     stages, refs = refs[:7], refs[7:]
-    (own_res, own_scales, res, scales, gains, mixes, after, normed, gate_buf, hidden, outgoing, from_x, to_z, from_z, to_x, whole_z,
+    (own_res, own_scales, res, scales, gains, mixes, after, normed, gate_buf, hidden, outgoing, from_x, to_z, from_z, to_x, whole_z, out_buf,
      raw_sem, z_send, z_recv, y_send, y_recv, t_send, t_recv, mx_send, mx_recv, mt_send, mt_recv,
      r_send, r_recv, s_send, s_recv, m_send, m_recv, px_send, px_recv, pz_send, pz_recv,
-     zz_send, zz_recv) = refs
+     zz_send, zz_recv, out_sem) = refs
     proj_buf, mout_buf, gate_w, up_w, down_w = bufs
     shards = gate_w.shape[0]
     place = lax.axis_index("fs")
@@ -254,9 +254,9 @@
     def spot(array, owner, half):
         if array == 1:
             return mout_buf.at[owner, group, half]
-        if array >= 4:
-            return down_w.at[owner, half, array - 4]
-        return bufs[array].at[owner, half]
+        if array >= 2:
+            return bufs[1 + array // 2].at[owner, half, array % 2]
+        return proj_buf.at[owner, half]
 
     def owner_of(r, far):
         return levels[r] * 2 + (1 - y if far else y)
@@ -386,22 +386,26 @@
     t_copy(1, 0, False).start()
     for copy in scale_copies:
         copy.start()
-    for array in (2, 3):
-        wait_raw(array + 2)
-        for target, cols in both(bufs[array].at[place, core], others[array - 1], width):
-            target[...] = stages[array + 2][:, cols].astype(jnp.bfloat16)
-        t_copy(array, 0, False).start()
-        if array == 2:
-            y_copy(2, 0).start()
-            start_z((2, 1))
-            start_inner((2, 2))
+    fine = rows // 2
+    for matrix in (1, 2):
+        wait_raw(matrix + 3)
+        for chunk in range(2):
+            array = 2 * matrix + chunk
+            lines = slice(chunk * fine, (chunk + 1) * fine)
+            for target, cols in both(spot(array, place, core), others[array - 1], width):
+                target[...] = stages[matrix + 3][lines, cols].astype(jnp.bfloat16)
+            t_copy(array, 0, False).start()
+            if matrix == 1:
+                y_copy(array, 0).start()
+                start_outer((array, 1))
+                start_inner((array, 2))
     wait_raw(6)
     short = tall // 2
-    for k, array in ((0, 4), (1, 5)):
-        lines = slice(k * short, (k + 1) * short)
-        down_w[place, core, k] = stages[6][part_of, lines, :].astype(jnp.bfloat16)
+    for chunk in range(2):
+        array = 6 + chunk
+        lines = slice(chunk * short, (chunk + 1) * short)
+        down_w[place, core, chunk] = stages[6][part_of, lines, :].astype(jnp.bfloat16)
         others[array - 1][...] = stages[6][1 - part_of, lines, :].astype(jnp.bfloat16)
-    for array in (4, 5):
         t_copy(array, 0, False).start()
     res[side, group] = own_res[...]
     scales[place] = own_scales[...]
@@ -462,14 +466,16 @@
     order = (1, 2, 3)
     take_z(0, 2)
     take_z(1, 2)
+    for array in (4, 5):
+        y_copy(array, 0).start()
     res_z.wait_recv()
     res_d.start()
-    start_inner((2, 3))
-    start_outer((2, 2))
+    start_inner((2, 3), (3, 3))
+    start_outer((2, 2), (3, 2))
     take_z(0, 1)
     take_z(0, 3)
-    y_copy(3, 0).start()
-    y_copy(4, 0).start()
+    for array in (6, 7):
+        y_copy(array, 0).start()
     res_x.wait_recv()
     normalize_side(side)
     for r in (0, 2, 1, 3):
@@ -499,15 +505,15 @@
     ]
     for copy in mix_copies:
         copy.start()
-    start_z((3, 1))
-    start_outer((3, 2))
+    start_inner((2, 1), (3, 1))
     start_z((4, 1), (5, 1))
+    start_outer((4, 2), (5, 2))
+    start_z((6, 1), (7, 1))
     each(
-        [("z", 1, 3), ("z", 2, 2), ("z", 1, 1), ("z", 2, 3), ("z", 2, 1)],
-        [("z", 1, 1), ("z", 1, 3), ("z", 2, 2), ("z", 2, 1)],
-    )
-    start_inner((3, 2), (3, 3))
-    y_copy(5, 0).start()
+        [("z", 1, 3), ("z", 2, 2), ("z", 2, 3), ("z", 1, 1), ("z", 3, 2), ("z", 3, 3)],
+        [("z", 1, 1), ("z", 1, 3), ("z", 2, 2), ("z", 3, 2), ("z", 2, 1), ("z", 3, 1),
+         ("s", 4, 2), ("s", 4, 3), ("s", 5, 2), ("s", 5, 3)],
+    )
     for r in (0, 2, 1, 3):
         take_y(1, r)
     for far in (False, True):
@@ -564,7 +570,7 @@
             body(whole * tile, width % tile)
 
     def multiply(weights, start, size):
-        weight = weights[:, :, :, pl.ds(start, size)].reshape(features, size)
+        weight = weights[:, :, :, :, pl.ds(start, size)].reshape(features, size)
         return jnp.dot(normed[...], weight, preferred_element_type=jnp.float32)
 
     def scale_at(scale, start, size):
@@ -584,19 +590,27 @@
             gate / (1.0 + jnp.exp(-gate)) * product
         ).astype(jnp.bfloat16)
 
-    each([], [("z", 2, 3), ("z", 3, 1)])
-    start_inner((4, 2), (5, 2))
-    for r in (0,) + order:
-        take_y(2, r)
+    each(
+        [("z", 2, 1), ("z", 3, 1), ("z", 4, 2), ("z", 4, 3)],
+        [("z", 2, 3), ("z", 3, 3), ("z", 4, 1), ("z", 5, 1), ("s", 6, 2), ("s", 7, 2)],
+    )
+    for array in (2, 3):
+        for r in (0,) + order:
+            take_y(array, r)
     finish(2)
+    finish(3)
     tiles(gate_tile)
     each(
-        [("z", 3, 2), ("z", 3, 3), ("s", 4, 2), ("s", 5, 2), ("z", 3, 1), ("z", 4, 1), ("z", 5, 1), ("y", 3, 0),
-         ("y", 3, 2), ("y", 3, 3), ("y", 3, 1)],
-        [("z", 3, 2), ("z", 3, 3), ("s", 4, 3), ("s", 5, 3), ("z", 4, 1), ("z", 5, 1), ("y", 3, 0), ("y", 3, 1),
-         ("y", 3, 2), ("z", 4, 2), ("z", 5, 2), ("y", 3, 3)],
-    )
-    finish(3)
+        [("z", 5, 2), ("z", 5, 3), ("s", 6, 2), ("s", 7, 2),
+         ("z", 4, 1), ("z", 5, 1), ("z", 6, 1), ("z", 7, 1),
+         ("y", 4, 0), ("y", 5, 0), ("y", 4, 2), ("y", 4, 3), ("y", 5, 2), ("y", 5, 3),
+         ("y", 4, 1), ("y", 5, 1)],
+        [("z", 4, 2), ("z", 5, 2), ("z", 4, 3), ("z", 5, 3), ("s", 6, 3), ("s", 7, 3),
+         ("z", 6, 1), ("z", 7, 1), ("y", 4, 0), ("y", 5, 0), ("y", 4, 1), ("y", 5, 1),
+         ("y", 4, 2), ("y", 5, 2), ("z", 6, 2), ("z", 7, 2), ("y", 4, 3), ("y", 5, 3)],
+    )
+    finish(4)
+    finish(5)
     tiles(up_tile)
 
     steps = [(r, far) for r in range(4) for far in (False, True)]
@@ -626,7 +640,7 @@
 
     def down(k):
         r, far = steps[k]
-        for array in (4, 5):
+        for array in (6, 7):
             t_copy(array, r, far).wait_recv()
         s = index_of(k)
         weight = down_w[s].reshape(width, block)
@@ -664,6 +678,11 @@
                 outgoing[k, 1 - side].astype(jnp.float32) + from_x[k, 1 - side].astype(jnp.float32)
             ).astype(jnp.bfloat16)
             pz_copy(k).start()
+
+    def out_copy(k):
+        i = slot_of(k)
+        target = out_ref.at[:, pl.ds(pl.multiple_of(i * block, block), block)]
+        return pltpu.make_async_copy(out_buf.at[i], target, out_sem.at[i])
 
     def close(k):
         i = slot_of(k)
@@ -677,15 +696,39 @@
             lines = pl.ds(pl.multiple_of(side * tokens, tokens), tokens)
             total = outgoing[k, side].astype(jnp.float32) + from_x[k, side].astype(jnp.float32)
             total = total + (whole_z[s] if k % 2 else from_z[i]).astype(jnp.float32)
-            out_ref[:, pl.ds(pl.multiple_of(i * block, block), block)] = (
-                after[s, lines, :].astype(jnp.float32) + total
-            ).astype(jnp.bfloat16)
+            out_buf[i] = (after[s, lines, :].astype(jnp.float32) + total).astype(jnp.bfloat16)
+            out_copy(k).start()
 
     def take_all(take, r):
-        for array in (4, 5):
+        for array in (6, 7):
             take(array, r)
 
-    each([("z", 4, 2), ("z", 5, 2)], [])
+    def early_waits():
+        z_copy(0, 3).wait_send()
+        z_copy(1, 3).wait_send()
+
+        @pl.when(inner)
+        def _():
+            for array in range(2, 8):
+                for way in (3, 4):
+                    z_copy(array, way).wait_send()
+
+        for array in range(8):
+            for r in range(4):
+                if r in (1, 2):
+                    z_copy(array, r).wait_send()
+                if array < 6 or r < 3:
+                    y_copy(array, r).wait_send()
+                    for far in (False, True):
+                        t_copy(array, r, far).wait_send()
+        for r in range(4):
+            for far in (False, True):
+                mx_copy(r, far).wait_send()
+                mt_copy(r, far).wait_send()
+        for copy in scale_copies + mix_copies + [res_z, res_x, res_d]:
+            copy.wait_send()
+
+    each([("z", 6, 2), ("z", 7, 2)], [])
     down(0)
     take_all(take_y, 0)
     down(1)
@@ -694,44 +737,31 @@
     down(3)
     down(4)
     take_all(take_z, 3)
-    pass_on(1)
     take_all(take_y, 2)
     down(5)
     down(6)
+    pass_on(1)
     pass_on(3)
     pass_on(0)
     pass_on(4)
+    early_waits()
+    take_y(6, 3)
+    pass_on(2)
+    take_y(7, 3)
+    down(7)
     pass_on(5)
-    take_all(take_y, 3)
-    down(7)
     pass_on(6)
-    pass_on(2)
+    close(0)
+    close(2)
+    close(4)
     pass_on(7)
-    for k in range(shards):
+    for k in (1, 3, 6, 5, 7):
         close(k)
 
-    z_copy(0, 3).wait_send()
-    z_copy(1, 3).wait_send()
-
-    @pl.when(inner)
-    def _():
-        for array in range(2, 6):
-            for way in (3, 4):
-                z_copy(array, way).wait_send()
-
-    for array in range(6):
-        for r in range(4):
-            if r in (1, 2):
-                z_copy(array, r).wait_send()
-            y_copy(array, r).wait_send()
-            for far in (False, True):
-                t_copy(array, r, far).wait_send()
-    for r in range(4):
-        for far in (False, True):
-            mx_copy(r, far).wait_send()
-            mt_copy(r, far).wait_send()
-    for copy in scale_copies + mix_copies + [res_z, res_x, res_d]:
-        copy.wait_send()
+    for array in (6, 7):
+        y_copy(array, 3).wait_send()
+        t_copy(array, 3, False).wait_send()
+        t_copy(array, 3, True).wait_send()
     for k in range(shards):
         if k % 2:
             zz_copy(k).wait_send()
@@ -743,6 +773,9 @@
             if k % 2 == 0:
                 px_copy(k, 0).wait_send()
             px_copy(k, 1).wait_send()
+
+    for k in range(shards):
+        pl.when(mine(k))(out_copy(k).wait)
 
 
 def fused(
@@ -765,16 +798,18 @@
         functools.partial(layer_kernel, channels, LEN),
         out_shape=jax.ShapeDtypeStruct((tokens, own_width), short),
         in_specs=[vmem] * (1 + len(small)) + [pl.BlockSpec(memory_space=pl.ANY)] * 7,
-        out_specs=vmem,
+        out_specs=pl.BlockSpec(memory_space=pl.ANY),
         scratch_shapes=[
             pltpu.VMEM((shards, 2, rows, 3 * narrow), short),
             pltpu.VMEM((shards, 2, 2, out_rows // 2, block), short),
-            pltpu.VMEM((shards, 2, rows, width), short),
-            pltpu.VMEM((shards, 2, rows, width), short),
+            pltpu.VMEM((shards, 2, 2, rows // 2, width), short),
+            pltpu.VMEM((shards, 2, 2, rows // 2, width), short),
             pltpu.VMEM((shards, 2, 2, tall // 2, block), short),
             pltpu.VMEM((rows, 3 * narrow), short),
-            pltpu.VMEM((rows, width), short),
-            pltpu.VMEM((rows, width), short),
+            pltpu.VMEM((rows // 2, width), short),
+            pltpu.VMEM((rows // 2, width), short),
+            pltpu.VMEM((rows // 2, width), short),
+            pltpu.VMEM((rows // 2, width), short),
             pltpu.VMEM((tall // 2, block), short),
             pltpu.VMEM((tall // 2, block), short),
         ]
@@ -800,13 +835,14 @@
             pltpu.VMEM((steps // 2, tokens, block), short),
             pltpu.VMEM((steps, tokens, block), short),
             pltpu.VMEM((steps, tokens, block), short),
+            pltpu.VMEM((steps // 2, tokens, block), short),
             dma((8,)),
-            dma((6, 4)),
-            dma((6, 3)),
-            dma((6, 4)),
-            dma((6, 4)),
-            dma((6, 8)),
-            dma((6, 8)),
+            dma((8, 4)),
+            dma((8, 3)),
+            dma((8, 4)),
+            dma((8, 4)),
+            dma((8, 8)),
+            dma((8, 8)),
             dma((8,)),
             dma((8,)),
             dma((8,)),
@@ -823,6 +859,7 @@
             dma((steps // 2,)),
             dma((steps,)),
             dma((steps,)),
+            dma((steps // 2,)),
         ],
         compiler_params=pltpu.CompilerParams(
             collective_id=1, has_side_effects=True, vmem_limit_bytes=60 * 1024 * 1024
@@ -867,7 +904,7 @@
     if (
         reps == 2 and groups == 2 and shards == 8 and tokens % LEN == 0
         and block % 128 == 0 and width % 256 == 0 and ff % 256 == 0 and block == width
-        and in_rows % 32 == 0 and out_rows == width and own_rows == block * shards // 2
+        and in_rows % 64 == 0 and out_rows == width and own_rows == block * shards // 2
     ):
         result = fused(
             shards, residual,

time: 145 us -> 143 us (0.986); the launches traced: 144 us -> 141 us
  Pallas kernels: 142 us -> 139 us
    pallas_call x1, Pallas kernels: 142 us -> 139 us  [fused(): pl.pallas_call(functools.partial(layer_kernel, channels, LEN), out_shape=...]
where the time goes in v2:
time: 143 us; the launch traced here: 141 us
  Pallas kernels  139 us (97%)
  local copies, waits for them, and re-layouts  2.04 us (1%)
    pallas_call x1, Pallas kernels, fused(): pl.pallas_call(functools.partial(layer_kernel, channels, LEN), out_shape=...  139 us

profile of v2, /device:TPU:0, one launch (start us, length us, event | category | flops | bytes accessed | tf_op | source)
XLA Modules:
  0.0 140.7 jit_solution(5303872183563267331)
XLA Ops:
  0.0 138.6 %layer.1 = bf16[256,1024]{1,0:T(8,128)(2,1)} custom-call(bf16[1024,256]{1,0:T(8,128)(2,1)} %residual.1, f32[1,2048]{1,0:T(1,128)} %bitcast.14, f32[1,256]{1,0:T(1,128)} %bitcast.16, f32[1,256]{1,0:T(1,128)} %bitcast.17, f32[1,256]{1,0:T(1,128)} %bitcast.18, f32[3,256]{1,0:T(4,128)} %taps.1, f32[1,256]{1,0:T(1,128)} %bitcast.19, f32[1,2048]{1,0:T(1,128)} %bitcast.15, ...), custom_call_target="tpu_custom_call" | custom-call | tf_op jit(solution)/shard_map/layer/pallas_call | solution.py:797
  138.6 2.0 %copy.20 = bf16[1024,256]{1,0:T(8,128)(2,1)} copy(bf16[1024,256]{0,1:T(8,128)(2,1)} %bitcast.11) | data formatting | bytes 1048576 | tf_op jit(solution)/shard_map/transpose | solution.py:917

commit v3 on v2

--- a/solution.py
+++ b/solution.py
@@ -397,7 +397,10 @@
             t_copy(array, 0, False).start()
             if matrix == 1:
                 y_copy(array, 0).start()
-                start_outer((array, 1))
+                if chunk == 0:
+                    start_z((array, 1))
+                else:
+                    start_outer((array, 1))
                 start_inner((array, 2))
     wait_raw(6)
     short = tall // 2
@@ -505,7 +508,7 @@
     ]
     for copy in mix_copies:
         copy.start()
-    start_inner((2, 1), (3, 1))
+    start_inner((3, 1))
     start_z((4, 1), (5, 1))
     start_outer((4, 2), (5, 2))
     start_z((6, 1), (7, 1))
@@ -520,6 +523,7 @@
         for r in range(4):
             mx_copy(r, far).wait_recv()
             mt_copy(r, far).start()
+    each([("z", 2, 1)], [])
     for copy in scale_copies + mix_copies:
         copy.wait_recv()
     finish(1)
@@ -591,7 +595,7 @@
         ).astype(jnp.bfloat16)
 
     each(
-        [("z", 2, 1), ("z", 3, 1), ("z", 4, 2), ("z", 4, 3)],
+        [("z", 4, 2), ("z", 4, 3), ("z", 3, 1), ("z", 5, 2), ("z", 5, 3)],
         [("z", 2, 3), ("z", 3, 3), ("z", 4, 1), ("z", 5, 1), ("s", 6, 2), ("s", 7, 2)],
     )
     for array in (2, 3):
@@ -601,7 +605,7 @@
     finish(3)
     tiles(gate_tile)
     each(
-        [("z", 5, 2), ("z", 5, 3), ("s", 6, 2), ("s", 7, 2),
+        [("s", 6, 2), ("s", 7, 2),
          ("z", 4, 1), ("z", 5, 1), ("z", 6, 1), ("z", 7, 1),
          ("y", 4, 0), ("y", 5, 0), ("y", 4, 2), ("y", 4, 3), ("y", 5, 2), ("y", 5, 3),
          ("y", 4, 1), ("y", 5, 1)],
@@ -624,19 +628,35 @@
     def slot_of(k):
         return lax.rem(index_of(k), per_group)
 
+    last = shards - 1
+    strip = tokens // 2
+
     def px_copy(k, which):
+        sems = px_send.at[k, which], px_recv.at[k, which], beside
+        if k == last:
+            lines = pl.ds(which * strip, strip)
+            return remote(to_x.at[k, lines], from_x.at[k, side, lines], *sems)
         who = 1 - side if which == 0 else side
-        return remote(
-            to_x.at[k] if k % 2 else outgoing.at[k, who], from_x.at[k, who], px_send.at[k, which], px_recv.at[k, which], beside
-        )
+        source = to_x.at[k] if k % 2 else outgoing.at[k, who]
+        return remote(source, from_x.at[k, who], *sems)
 
     def pz_copy(k):
         i = slot_of(k)
         return remote(to_z.at[i], from_z.at[i], pz_send.at[i], pz_recv.at[i], mate)
 
-    def zz_copy(k):
+    def zz_copies(k):
         s = index_of(k)
-        return remote(outgoing.at[k, 1 - side], whole_z.at[s], zz_send.at[s], zz_recv.at[s], mate)
+        mates = outgoing.at[k, 1 - side]
+        if k < last:
+            return [remote(mates, whole_z.at[s], zz_send.at[s], zz_recv.at[s], mate)]
+        copies = []
+        for half, index in ((0, s), (1, shards)):
+            lines = pl.ds(half * strip, strip)
+            copies.append(remote(
+                outgoing.at[k, 1 - side, lines], whole_z.at[s, lines],
+                zz_send.at[index], zz_recv.at[index], mate,
+            ))
+        return copies
 
     def down(k):
         r, far = steps[k]
@@ -650,7 +670,8 @@
         outgoing[k, 1] = part[tokens:]
 
         if k % 2:
-            zz_copy(k).start()
+            for copy in zz_copies(k):
+                copy.start()
             return
 
         @pl.when(jnp.logical_not(mine(k)))
@@ -660,14 +681,19 @@
 
     def pass_on(k):
         if k % 2:
-            zz_copy(k).wait_recv()
-
-            @pl.when(jnp.logical_not(mine(k)))
-            def _():
-                to_x[k] = (
-                    outgoing[k, side].astype(jnp.float32) + whole_z[index_of(k)].astype(jnp.float32)
-                ).astype(jnp.bfloat16)
-                px_copy(k, 1).start()
+            copies = zz_copies(k)
+            for which, copy in enumerate(copies):
+                copy.wait_recv()
+                size = tokens // len(copies)
+                lines = slice(which * size, (which + 1) * size)
+
+                @pl.when(jnp.logical_not(mine(k)))
+                def _():
+                    to_x[k, lines] = (
+                        outgoing[k, side, lines].astype(jnp.float32)
+                        + whole_z[index_of(k), lines].astype(jnp.float32)
+                    ).astype(jnp.bfloat16)
+                    px_copy(k, which if k == last else 1).start()
 
             return
 
@@ -691,6 +717,8 @@
         @pl.when(mine(k))
         def _():
             px_copy(k, 1).wait_recv()
+            if k == last:
+                px_copy(k, 0).wait_recv()
             if k % 2 == 0:
                 pz_copy(k).wait_recv()
             lines = pl.ds(pl.multiple_of(side * tokens, tokens), tokens)
@@ -734,9 +762,10 @@
     down(1)
     down(2)
     take_all(take_y, 1)
+    each([("z", 6, 3), ("z", 7, 3)], [])
     down(3)
     down(4)
-    take_all(take_z, 3)
+    each([], [("z", 6, 3), ("z", 7, 3)])
     take_all(take_y, 2)
     down(5)
     down(6)
@@ -764,13 +793,14 @@
         t_copy(array, 3, True).wait_send()
     for k in range(shards):
         if k % 2:
-            zz_copy(k).wait_send()
+            for copy in zz_copies(k):
+                copy.wait_send()
         else:
             pl.when(mine(k))(pz_copy(k).wait_send)
 
         @pl.when(jnp.logical_not(mine(k)))
         def _():
-            if k % 2 == 0:
+            if k % 2 == 0 or k == last:
                 px_copy(k, 0).wait_send()
             px_copy(k, 1).wait_send()
 
@@ -857,8 +887,8 @@
             dma((steps, 2)),
             dma((steps // 2,)),
             dma((steps // 2,)),
-            dma((steps,)),
-            dma((steps,)),
+            dma((steps + 1,)),
+            dma((steps + 1,)),
             dma((steps // 2,)),
         ],
         compiler_params=pltpu.CompilerParams(

time: 143 us -> 141 us (0.986)
  no operation moved by 1% of the time
where the time goes in v3:
time: 141 us; the launch traced here: 140 us
  Pallas kernels  138 us (98%)
  local copies, waits for them, and re-layouts  2.04 us (1%)
    pallas_call x1, Pallas kernels, fused(): pl.pallas_call(functools.partial(layer_kernel, channels, LEN), out_shape=...  138 us

profile of v3, /device:TPU:0, one launch (start us, length us, event | category | flops | bytes accessed | tf_op | source)
XLA Modules:
  0.0 139.7 jit_solution(10693919247162561122)
XLA Ops:
  0.0 137.7 %layer.1 = bf16[256,1024]{1,0:T(8,128)(2,1)} custom-call(bf16[1024,256]{1,0:T(8,128)(2,1)} %residual.1, f32[1,2048]{1,0:T(1,128)} %bitcast.14, f32[1,256]{1,0:T(1,128)} %bitcast.16, f32[1,256]{1,0:T(1,128)} %bitcast.17, f32[1,256]{1,0:T(1,128)} %bitcast.18, f32[3,256]{1,0:T(4,128)} %taps.1, f32[1,256]{1,0:T(1,128)} %bitcast.19, f32[1,2048]{1,0:T(1,128)} %bitcast.15, ...), custom_call_target="tpu_custom_call" | custom-call | tf_op jit(solution)/shard_map/layer/pallas_call | solution.py:827
  137.7 2.0 %copy.20 = bf16[1024,256]{1,0:T(8,128)(2,1)} copy(bf16[1024,256]{0,1:T(8,128)(2,1)} %bitcast.11) | data formatting | bytes 1048576 | tf_op jit(solution)/shard_map/transpose | solution.py:947

commit v4 on v3

--- a/solution.py
+++ b/solution.py
@@ -677,7 +677,9 @@
         @pl.when(jnp.logical_not(mine(k)))
         def _():
             px_copy(k, 0).start()
-            px_copy(k, 1).start()
+            if k % per_group:
+                px_copy(k - 2, 1).start()
+                px_copy(k, 1).start()
 
     def pass_on(k):
         if k % 2:

time: 141 us -> 141 us (level)
  no operation moved by 1% of the time
where the time goes in v4:
time: 141 us; the launch traced here: 140 us
  Pallas kernels  138 us (98%)
  local copies, waits for them, and re-layouts  2.04 us (1%)
    pallas_call x1, Pallas kernels, fused(): pl.pallas_call(functools.partial(layer_kernel, channels, LEN), out_shape=...  138 us

profile of v4, /device:TPU:0, one launch (start us, length us, event | category | flops | bytes accessed | tf_op | source)
XLA Modules:
  0.0 139.9 jit_solution(17308783515325071785)
XLA Ops:
  0.0 137.9 %layer.1 = bf16[256,1024]{1,0:T(8,128)(2,1)} custom-call(bf16[1024,256]{1,0:T(8,128)(2,1)} %residual.1, f32[1,2048]{1,0:T(1,128)} %bitcast.14, f32[1,256]{1,0:T(1,128)} %bitcast.16, f32[1,256]{1,0:T(1,128)} %bitcast.17, f32[1,256]{1,0:T(1,128)} %bitcast.18, f32[3,256]{1,0:T(4,128)} %taps.1, f32[1,256]{1,0:T(1,128)} %bitcast.19, f32[1,2048]{1,0:T(1,128)} %bitcast.15, ...), custom_call_target="tpu_custom_call" | custom-call | tf_op jit(solution)/shard_map/layer/pallas_call | solution.py:829
  137.9 2.0 %copy.20 = bf16[1024,256]{1,0:T(8,128)(2,1)} copy(bf16[1024,256]{0,1:T(8,128)(2,1)} %bitcast.11) | data formatting | bytes 1048576 | tf_op jit(solution)/shard_map/transpose | solution.py:949
